TPU v7x, 32 devices: a whole 2x2x4 slice. The times are simulated.
32 devices in a mesh: sp: 8 (over z, y), tp: 4 (over x, core).
Axes of the slice: x: 2, y: 2, z: 4, core: 2. Of those that a mesh axis runs over, the one named last changes fastest.
Arguments:
- query_rows: bfloat16 [4096, 2048], P('sp', 'tp'), may hold values from -40 to 40
- key_rows: bfloat16 [4096, 256], P('sp', 'tp'), may hold values from -6 to 6
- value_rows: bfloat16 [4096, 256], P('sp', 'tp'), may hold values from -12 to 12
- doc_ids: int32 [4096], P('sp'), may hold values from 0 to 3, never falling along the last dimension, each value on 1 to 2048 neighbouring positions
- sink_logit: float32 [32], P('tp'), may hold values from 1 to 6
- residual: bfloat16 [4096, 2048], P('sp'), may hold values from -10 to 10
- out_proj: bfloat16 [2048, 2048], P('tp'), may hold values from -0.25 to 0.25
- mix_gain: float32 [2048], replicated, may hold values from 0.1 to 1.9
- gate_proj: bfloat16 [2048, 5632], P('sp', 'tp'), may hold values from -0.125 to 0.125
- value_proj: bfloat16 [2048, 5632], P('sp', 'tp'), may hold values from -0.125 to 0.125
- gate_taps: float32 [3, 5632], P(None, 'tp'), may hold values from -3 to 3
- value_taps: float32 [3, 5632], P(None, 'tp'), may hold values from -3 to 3
- down_proj: bfloat16 [5632, 2048], P('tp', 'sp'), may hold values from -0.078125 to 0.078125
- final_gain: float32 [2048], P('tp'), may hold values from 0.1 to 1.9
Outputs:
- mixed: bfloat16 [4096, 2048], P('sp', 'tp')
All inputs are finite; a program needn't handle non-finite values.
Results may differ from a plain program's by a relative error of at most 0.012.
Values may be sent and summed in bfloat16 or wider, within the bound.
A program may use at most 128 MiB of HBM per device.

v0:
```python
import math
import jax
import jax.numpy as jnp
from jax import lax
from jax.sharding import PartitionSpec as P

HD = 64
WIN = 128
TAPS = 3
mix_scale = math.sqrt(2.0)
norm_eps = 1e-05


def passed_along(block, axis, distance):
    devices = range(lax.axis_size(axis))
    route = [(i - distance, i) for i in devices if i - distance in devices]
    return lax.ppermute(block, axis, route)


def attend(query_block, key_block, value_block, query_pos, key_pos, query_doc, key_doc, sink):
    head_size = query_block.shape[-1]
    scores = jnp.einsum(
        "qkgd,skd->kgqs", query_block, key_block, preferred_element_type=jnp.float32
    ) * head_size ** (-0.5)
    diff = query_pos[:, None] - key_pos[None, :]
    valid = (
        (diff >= 0)
        & (diff < WIN)
        & (query_doc[:, None] == key_doc[None, :])
        & (key_pos[None, :] >= 0)
    )
    scores = jnp.where(valid[None, None], scores, -1e30)
    top = jnp.maximum(jnp.max(scores, axis=-1, keepdims=True), sink)
    weights = jnp.exp(scores - top)
    total = jnp.sum(weights, axis=-1, keepdims=True) + jnp.exp(sink - top)
    probs = (weights / total).astype(jnp.bfloat16)
    out = jnp.einsum("kgqs,skd->qkgd", probs, value_block, preferred_element_type=jnp.float32)
    return out.astype(jnp.bfloat16)


def depthwise(tail, current, taps, tail_docs, docs):
    extended = jnp.concatenate([tail, current])
    ext_docs = jnp.concatenate([tail_docs, docs])
    lag_rows = tail.shape[0]
    count = current.shape[0]
    total = jnp.zeros(current.shape, jnp.float32)
    for lag in range(lag_rows + 1):
        start = lag_rows - lag
        same = (ext_docs[start : start + count] == docs)[:, None]
        rows = extended[start : start + count].astype(jnp.float32)
        total = total + taps[lag][None, :] * jnp.where(same, rows, 0.0)
    return total


def on_device(
    query_rows,
    key_rows,
    value_rows,
    doc_ids,
    sink_logit,
    residual,
    out_proj,
    mix_gain,
    gate_proj,
    value_proj,
    gate_taps,
    value_taps,
    down_proj,
    final_gain,
):
    rows = query_rows.shape[0]
    kv_local = key_rows.shape[1] // HD
    heads_local = query_rows.shape[1] // HD
    groups = heads_local // kv_local
    offset = lax.axis_index("sp") * rows
    prev_keys, prev_values, prev_docs = passed_along(
        (key_rows[rows - WIN :], value_rows[rows - WIN :], doc_ids[rows - WIN :]), "sp", 1
    )
    all_keys = jnp.concatenate([prev_keys, key_rows]).reshape(rows + WIN, kv_local, HD)
    all_values = jnp.concatenate([prev_values, value_rows]).reshape(rows + WIN, kv_local, HD)
    all_docs = jnp.concatenate([prev_docs, doc_ids])
    key_pos = offset - WIN + jnp.arange(rows + WIN, dtype=jnp.int32)
    query_pos = offset + jnp.arange(rows, dtype=jnp.int32)
    queries = query_rows.reshape(rows, kv_local, groups, HD)
    sink = sink_logit.reshape(kv_local, groups, 1, 1)
    pieces = attend(queries, all_keys, all_values, query_pos, key_pos, doc_ids, all_docs, sink)
    heads = pieces.reshape(rows, heads_local * HD)
    partial_value = jnp.dot(heads, out_proj, preferred_element_type=jnp.float32)
    width = residual.shape[1]
    share = width // lax.axis_size("tp")
    col_start = lax.axis_index("tp") * share
    attn_total = lax.psum(partial_value.astype(jnp.bfloat16), "tp").astype(jnp.float32)
    first_sum = mix_scale * residual.astype(jnp.float32) + attn_total
    mean = jnp.mean(first_sum, axis=1, keepdims=True)
    var = jnp.mean(jnp.square(first_sum - mean), axis=1, keepdims=True)
    normed = ((first_sum - mean) * lax.rsqrt(var + norm_eps) * mix_gain[None, :]).astype(
        jnp.bfloat16
    )
    normed_own = lax.dynamic_slice_in_dim(normed, col_start, share, 1)
    up_gate = jnp.dot(
        normed,
        lax.all_gather(gate_proj, "sp", axis=0, tiled=True),
        preferred_element_type=jnp.float32,
    )
    up_value = jnp.dot(
        normed,
        lax.all_gather(value_proj, "sp", axis=0, tiled=True),
        preferred_element_type=jnp.float32,
    )
    up_gate = up_gate.astype(jnp.bfloat16)
    up_value = up_value.astype(jnp.bfloat16)
    lag_rows = TAPS - 1
    prev_gate, prev_value = passed_along(
        (up_gate[rows - lag_rows :], up_value[rows - lag_rows :]), "sp", 1
    )
    tail_docs = prev_docs[WIN - lag_rows :]
    conv_gate = depthwise(prev_gate, up_gate, gate_taps, tail_docs, doc_ids)
    conv_value = depthwise(prev_value, up_value, value_taps, tail_docs, doc_ids)
    hidden = (jax.nn.gelu(conv_gate) * conv_value).astype(jnp.bfloat16)
    terms = jnp.dot(
        hidden,
        lax.all_gather(down_proj, "sp", axis=1, tiled=True),
        preferred_element_type=jnp.float32,
    )
    ffn_own = lax.psum_scatter(
        terms.astype(jnp.bfloat16), "tp", scatter_dimension=1, tiled=True
    ).astype(jnp.float32)
    second_sum = mix_scale * normed_own.astype(jnp.float32) + ffn_own
    row_sum, row_squares = lax.psum(
        (jnp.sum(second_sum, axis=1), jnp.sum(second_sum * second_sum, axis=1)), "tp"
    )
    mean = row_sum / width
    var = row_squares / width - mean * mean
    return (
        (second_sum - mean[:, None]) * lax.rsqrt(var + norm_eps)[:, None] * final_gain[None, :]
    ).astype(jnp.bfloat16)


def solution(mesh):
    placed = (
        P("sp", "tp"),
        P("sp", "tp"),
        P("sp", "tp"),
        P("sp"),
        P("tp"),
        P("sp", None),
        P("tp", None),
        P(),
        P("sp", "tp"),
        P("sp", "tp"),
        P(None, "tp"),
        P(None, "tp"),
        P("tp", "sp"),
        P("tp"),
    )
    return jax.shard_map(
        on_device, mesh=mesh, in_specs=placed, out_specs=P("sp", "tp"), check_vma=False
    )
```

profile of v0, /device:TPU:0, one launch (start us, length us, event | category | flops | bytes accessed | tf_op | source)
XLA Modules:
  0.0 373.8 jit_solution(1086754709857433635)
XLA Ops:
  7.4 0.0 copy-start
  7.4 0.0 all-reduce.3.cloned.1.call-start
  7.4 0.8 slice.57
  8.2 4.9 %collective-permute-start.1 = (s32[128]{0:T(128)S(1)}, s32[128]{0:T(128)S(1)}, u32[]{:S(2)}, u32[]{:S(2)}) collective-permute-start(s32[128]{0:T(128)S(1)} %slice.57), channel_id=1, source_target_pairs={{0,4},{4,8},{8,12},{12,16},{16,20},{20,24},{24,28},{1,5},{5,9},{9,... | collective-permute-start | bytes 1544 | tf_op jit(solution)/shard_map/ppermute | solution.py:17
  13.1 0.7 slice.58
  13.8 3.4 collective-permute-start.2
  17.2 0.7 slice.56
  18.0 3.4 collective-permute-start
  21.4 1.3 copy.17
  22.7 0.0 collective-permute-done.1
  22.7 0.7 pad_add_fusion
  23.4 1.4 fusion.21
  24.8 0.0 collective-permute-done.2
  24.8 0.0 copy-start.9
  24.8 2.6 fusion.1
  27.4 0.0 copy-done.9
  27.4 0.1 broadcast_maximum_fusion
  27.5 2.1 fusion
  29.6 0.1 exponential_add_fusion
  29.7 0.0 collective-permute-done
  29.7 0.0 copy-done.7
  29.7 3.1 fusion.22
  32.9 0.0 copy-done
  32.9 2.6 convolution_convert_fusion.2
  35.5 0.0 all-reduce.3.cloned.1.call-update
  35.5 0.0 all-gather.4.cloned.1.call-start
  35.6 0.5 all-gather.4.cloned.1.call-update
  36.1 0.0 all-gather.6.cloned.1.call-start
  36.1 0.5 all-gather.6.cloned.1.call-update
  36.7 0.0 all-gather.8.cloned.1.call-start
  36.7 0.5 all-gather.8.cloned.1.call-update
  37.2 0.2 reduce-scatter.2.cloned.1.call-start
  37.5 0.0 copy-done.4
  37.5 0.0 copy-done.5
  37.5 0.1 slice_reduce_fusion.2
  37.6 0.1 slice.61
  37.7 0.0 copy-done.3
  37.7 0.1 pad_add_fusion.1
  37.7 48.6 %all-reduce.3.cloned.1.call-done = bf16[512,2048]{1,0:T(8,128)(2,1)} async-done(((bf16[512,2048]{1,0:T(8,128)(2,1)}), bf16[512,2048]{1,0:T(8,128)(2,1)}) %all-reduce.3.cloned.1.call-update) | async-done | bytes 2097168 | tf_op jit(solution)/shard_map/psum | solution.py:92
  86.3 3.1 fusion.4
  89.5 0.0 copy-done.1
  89.5 0.4 copy-done.2
  89.8 1.0 multiply_reduce_fusion
  90.8 0.0 copy-done.6
  90.9 2.4 multiply_convert_fusion
  93.2 36.4 %all-gather.4.cloned.1.call-done = bf16[2048,1408]{1,0:T(8,128)(2,1)} async-done(((bf16[256,1408]{1,0:T(8,128)(2,1)}), bf16[2048,1408]{1,0:T(8,128)(2,1)}) %all-gather.4.cloned.1.call-update) | async-done | bytes 5767184 | tf_op jit(solution)/shard_map/all_gather | solution.py:102
  129.6 6.7 %convolution_convert_fusion.1 = bf16[512,1408]{1,0:T(8,128)(2,1)S(1)} fusion(bf16[512,2048]{1,0:T(8,128)(2,1)} %multiply_convert_fusion, bf16[2048,1408]{1,0:T(8,128)(2,1)} %all-gather.4.cloned.1.call-done), kind=kOutput, calls=%fused_computation.13 | convolution fusion | flops 2953510912 | bytes 9306112 | tf_op jit(solution)/shard_map/dot_general | solution.py:100
  136.3 0.0 copy-start.10
  136.3 1.1 copy-done.10
  137.5 2.5 collective-permute-start.3
  139.9 82.1 %all-gather.6.cloned.1.call-done = bf16[2048,1408]{1,0:T(8,128)(2,1)} async-done(((bf16[256,1408]{1,0:T(8,128)(2,1)}), bf16[2048,1408]{1,0:T(8,128)(2,1)}) %all-gather.6.cloned.1.call-update) | async-done | bytes 5767184 | tf_op jit(solution)/shard_map/all_gather | solution.py:107
  222.0 6.7 %convolution_convert_fusion = bf16[512,1408]{1,0:T(8,128)(2,1)S(1)} fusion(bf16[512,2048]{1,0:T(8,128)(2,1)} %multiply_convert_fusion, bf16[2048,1408]{1,0:T(8,128)(2,1)} %all-gather.6.cloned.1.call-done), kind=kOutput, calls=%fused_computation.12 | convolution fusion | flops 2953510912 | bytes 9306112 | tf_op jit(solution)/shard_map/dot_general | solution.py:105
  228.7 0.0 copy-start.11
  228.7 2.5 collective-permute-start.4
  231.2 0.1 slice_compare_fusion.1
  231.3 83.8 %all-gather.8.cloned.1.call-done = bf16[1408,2048]{1,0:T(8,128)(2,1)} async-done(((bf16[1408,256]{1,0:T(8,128)(2,1)}), bf16[1408,2048]{1,0:T(8,128)(2,1)}) %all-gather.8.cloned.1.call-update) | async-done | bytes 5767184 | tf_op jit(solution)/shard_map/all_gather | solution.py:122
  315.1 0.0 collective-permute-done.3
  315.1 0.0 collective-permute-done.4
  315.1 12.0 %convolution_convert_fusion.3 = bf16[512,2048]{1,0:T(8,128)(2,1)} fusion(bf16[1408,2048]{1,0:T(8,128)(2,1)} %all-gather.8.cloned.1.call-done, bf16[512,1408]{1,0:T(8,128)(2,1)} %copy-done.11, bf16[512,1408]{1,0:T(8,128)(2,1)} %copy-done.10, bf16[2,1408]{1,0:T(2,128)(2,1)S(1)} %collective-permute-done.4, bf16[2,1408]{1,0:T(2,128)(2,1)S(1)} %collective-permute-done.3, ...), kind=kOutput, calls=%fused_computation.15 | convolution fusion | flops 2984116224 | bytes 10793984 | tf_op jit(solution)/shard_map/dot_general | solution.py:120
  327.1 0.0 reduce-scatter.2.cloned.1.call-update
  327.1 29.5 %reduce-scatter.2.cloned.1.call-done = bf16[512,512]{1,0:T(8,128)(2,1)} async-done(((bf16[512,2048]{1,0:T(8,128)(2,1)}), bf16[512,512]{1,0:T(8,128)(2,1)}) %reduce-scatter.2.cloned.1.call-update) | async-done | bytes 524304 | tf_op jit(solution)/shard_map/reduce_scatter | solution.py:125
  356.6 1.5 fusion.25
  358.2 5.8 %all-reduce = (f32[512]{0:T(512)S(1)}, f32[512]{0:T(512)S(1)}) all-reduce(f32[512]{0:T(512)S(1)} %get-tuple-element.6, f32[512]{0:T(512)S(1)} %get-tuple-element.5), channel_id=1, replica_groups=mesh['sp'=8,'tp'=4] {'tp'}, use_global_device_ids=true, to_apply=%region_9.10 | all-reduce | flops 1024 | bytes 8192 | tf_op jit(solution)/shard_map/psum | solution.py:129
  363.9 2.3 multiply_convert_fusion.1
  (18 shorter events, 0.1 us)
Async XLA Ops:
  7.4 25.5 %copy-start = (bf16[512,2048]{1,0:T(8,128)(2,1)S(1)}, bf16[512,2048]{1,0:T(8,128)(2,1)}, u32[]{:S(2)}) copy-start(bf16[512,2048]{1,0:T(8,128)(2,1)} %param.20) | copy-start | bytes 6291460
  7.4 78.9 %all-reduce.3.cloned.1.call-start = ((), (), s32[]{:S(2)}) async-start(), calls=%async_computation.1 | async-start | bytes 4194304 | tf_op jit(solution)/shard_map/psum | solution.py:92
  8.2 14.5 %collective-permute-start.1 = (s32[128]{0:T(128)S(1)}, s32[128]{0:T(128)S(1)}, u32[]{:S(2)}, u32[]{:S(2)}) collective-permute-start(s32[128]{0:T(128)S(1)} %slice.57), channel_id=1, source_target_pairs={{0,4},{4,8},{8,12},{12,16},{16,20},{20,24},{24,28},{1,5},{5,9},{9,... | collective-permute-start | bytes 1544 | tf_op jit(solution)/shard_map/ppermute | solution.py:17
  13.8 11.0 %collective-permute-start.2 = (bf16[128,64]{0,1:T(8,128)(2,1)S(1)}, bf16[128,64]{0,1:T(8,128)(2,1)S(1)}, u32[]{:S(2)}, u32[]{:S(2)}) collective-permute-start(bf16[128,64]{0,1:T(8,128)(2,1)S(1)} %slice.58), channel_id=1, source_target_pairs={{0,4},{4,8},{8,12},{12,16},{16,20},{20,24},{24,28},{1,5},{5,9},{9,... | collective-permute-start | bytes 49160 | tf_op jit(solution)/shard_map/ppermute | solution.py:17
  18.0 11.7 %collective-permute-start = (bf16[128,64]{0,1:T(8,128)(2,1)S(1)}, bf16[128,64]{0,1:T(8,128)(2,1)S(1)}, u32[]{:S(2)}, u32[]{:S(2)}) collective-permute-start(bf16[128,64]{0,1:T(8,128)(2,1)S(1)} %slice.56), channel_id=1, source_target_pairs={{0,4},{4,8},{8,12},{12,16},{16,20},{20,24},{24,28},{1,5},{5,9},{9,... | collective-permute-start | bytes 49160 | tf_op jit(solution)/shard_map/ppermute | solution.py:17
  24.8 2.6 copy-start.9
  27.5 2.2 copy-start.7
  35.5 2.0 copy-start.4
  35.5 2.0 copy-start.5
  35.5 2.2 copy-start.3
  35.5 94.1 %all-gather.4.cloned.1.call-start = ((), (), s32[]{:S(2)}) async-start(), calls=%async_computation.2 | async-start | bytes 6488064 | tf_op jit(solution)/shard_map/all_gather | solution.py:102
  36.1 185.9 %all-gather.6.cloned.1.call-start = ((), (), s32[]{:S(2)}) async-start(), calls=%async_computation.3 | async-start | bytes 6488064 | tf_op jit(solution)/shard_map/all_gather | solution.py:107
  36.7 278.4 %all-gather.8.cloned.1.call-start = ((), (), s32[]{:S(2)}) async-start(), calls=%async_computation.4 | async-start | bytes 6488064 | tf_op jit(solution)/shard_map/all_gather | solution.py:122
  37.2 319.4 %reduce-scatter.2.cloned.1.call-start = ((), (), s32[]{:S(2)}) async-start(), calls=%async_computation.5 | async-start | bytes 2621440 | tf_op jit(solution)/shard_map/reduce_scatter | solution.py:125
  86.3 3.1 copy-start.1
  86.3 3.5 copy-start.2
  89.4 1.4 copy-start.6
  136.3 1.1 copy-start.10
  137.5 177.6 %collective-permute-start.3 = (bf16[2,1408]{1,0:T(2,128)(2,1)S(1)}, bf16[2,1408]{1,0:T(2,128)(2,1)S(1)}, u32[]{:S(2)}, u32[]{:S(2)}) collective-permute-start(bf16[2,1408]{1,0:T(2,128)(2,1)S(1)} %slice.74), channel_id=1, source_target_pairs={{0,4},{4,8},{8,12},{12,16},{16,20},{20,24},{24,28},{1,5},{5,9},{9,... | collective-permute-start | bytes 16904 | tf_op jit(solution)/shard_map/ppermute | solution.py:17
  228.7 2.5 copy-start.11
  228.7 86.3 %collective-permute-start.4 = (bf16[2,1408]{1,0:T(2,128)(2,1)S(1)}, bf16[2,1408]{1,0:T(2,128)(2,1)S(1)}, u32[]{:S(2)}, u32[]{:S(2)}) collective-permute-start(bf16[2,1408]{1,0:T(2,128)(2,1)S(1)} %slice.77), channel_id=1, source_target_pairs={{0,4},{4,8},{8,12},{12,16},{16,20},{20,24},{24,28},{1,5},{5,9},{9,... | collective-permute-start | bytes 16904 | tf_op jit(solution)/shard_map/ppermute | solution.py:17
  327.1 36.8 %copy-start.8 = (f32[512]{0:T(512)S(1)}, f32[512]{0:T(512)}, u32[]{:S(2)}) copy-start(f32[512]{0:T(512)} %param.27) | copy-start | bytes 6148
Sparse Core Ops, SparseCore 0:
  35.6 50.6 all-reduce.2
  327.2 29.3 reduce-scatter.1
Sparse Core Ops, SparseCore 1:
  38.2 91.4 all-gather.3
  131.7 90.3 all-gather.5
  223.9 91.1 all-gather.7
where the time goes:
time: 374 us
  waiting for transfers between devices  282 us (75%)
  matrix products  33.7 us (9%)
  starting transfers between devices  17 us (5%)
  between operations  15.3 us (4%)
  other arithmetic  14.9 us (4%)
  blocking collectives  5.76 us (2%)
  local copies, waits for them, and re-layouts  5.23 us (1%)
    all_gather x1, waiting for transfers between devices, on_device(): lax.all_gather(down_proj, 'sp', axis=1, tiled=True)  83.8 us
    all_gather x1, waiting for transfers between devices, on_device(): lax.all_gather(value_proj, 'sp', axis=0, tiled=True)  82.1 us
    psum x1, waiting for transfers between devices, on_device(): lax.psum(partial_value.astype(jnp.bfloat16), 'tp').astype(jnp.float32)  48.6 us
    all_gather x1, waiting for transfers between devices, on_device(): lax.all_gather(gate_proj, 'sp', axis=0, tiled=True)  36.4 us
    reduce_scatter x1, waiting for transfers between devices, on_device(): lax.psum_scatter(terms.astype(jnp.bfloat16), 'tp', scatter_dimension=1, t...  29.5 us
    ppermute x5, starting transfers between devices, passed_along(): return lax.ppermute(block, axis, route)  16.6 us
    dot_general x1, matrix products, on_device(): jnp.dot(hidden, lax.all_gather(down_proj, 'sp', axis=1, tiled=True), pref...  12 us
  transfers between devices with their start and end apart: 10, of which 5 were waited for; matrix products, arithmetic and copies ran while one was open for 8% of the time, Pallas kernels for 0%

commit v1 on v0

--- a/solution.py
+++ b/solution.py
@@ -89,7 +89,9 @@
     width = residual.shape[1]
     share = width // lax.axis_size("tp")
     col_start = lax.axis_index("tp") * share
-    attn_total = lax.psum(partial_value.astype(jnp.bfloat16), "tp").astype(jnp.float32)
+    attn_total = jnp.sum(lax.all_gather(partial_value.astype(jnp.bfloat16), "tp"), axis=0).astype(
+        jnp.float32
+    )
     first_sum = mix_scale * residual.astype(jnp.float32) + attn_total
     mean = jnp.mean(first_sum, axis=1, keepdims=True)
     var = jnp.mean(jnp.square(first_sum - mean), axis=1, keepdims=True)

time: 374 us -> 431 us (1.15)
  waiting for transfers between devices: 282 us -> 333 us
  other arithmetic: 14.9 us -> 22.3 us
    all_gather x0 -> x1, waiting for transfers between devices: none -> 55.1 us  [on_device(): lax.all_gather(partial_value.astype(jnp.bfloat16), 'tp')]
    psum x1 -> x0, waiting for transfers between devices: 48.6 us -> none  [on_device(): lax.psum(partial_value.astype(jnp.bfloat16), 'tp').astype(jnp.float32)]
    all_gather x1, waiting for transfers between devices: 36.4 us -> 79.9 us  [on_device(): lax.all_gather(gate_proj, 'sp', axis=0, tiled=True)]
    reduce_sum x0 -> x1, other arithmetic: none -> 7.25 us  [on_device(): jnp.sum(lax.all_gather(partial_value.astype(jnp.bfloat16), 'tp'), axis=0)]
  transfers between devices with their start and end apart: 10 -> 10, of which waited for: 5 -> 5; matrix products, arithmetic and copies ran while one was open for 8% -> 9% of each run, Pallas kernels for 0% -> 0%
where the time goes in v1:
time: 431 us
  waiting for transfers between devices  333 us (77%)
  matrix products  33.8 us (8%)
  other arithmetic  22.3 us (5%)
  starting transfers between devices  17.2 us (4%)
  between operations  13.4 us (3%)
  blocking collectives  5.76 us (1%)
  local copies, waits for them, and re-layouts  5.53 us (1%)
    all_gather x1, waiting for transfers between devices, on_device(): lax.all_gather(down_proj, 'sp', axis=1, tiled=True)  83.8 us
    all_gather x1, waiting for transfers between devices, on_device(): lax.all_gather(value_proj, 'sp', axis=0, tiled=True)  82.5 us
    all_gather x1, waiting for transfers between devices, on_device(): lax.all_gather(gate_proj, 'sp', axis=0, tiled=True)  79.9 us
    all_gather x1, waiting for transfers between devices, on_device(): lax.all_gather(partial_value.astype(jnp.bfloat16), 'tp')  55.1 us
    reduce_scatter x1, waiting for transfers between devices, on_device(): lax.psum_scatter(terms.astype(jnp.bfloat16), 'tp', scatter_dimension=1, t...  29.5 us
    ppermute x5, starting transfers between devices, passed_along(): return lax.ppermute(block, axis, route)  16.9 us
    dot_general x1, matrix products, on_device(): jnp.dot(hidden, lax.all_gather(down_proj, 'sp', axis=1, tiled=True), pref...  12.1 us
  transfers between devices with their start and end apart: 10, of which 5 were waited for; matrix products, arithmetic and copies ran while one was open for 9% of the time, Pallas kernels for 0%

profile of v1, /device:TPU:0, one launch (start us, length us, event | category | flops | bytes accessed | tf_op | source)
XLA Modules:
  0.0 430.8 jit_solution(1563224913976553067)
XLA Ops:
  6.5 0.0 copy-start
  6.5 0.0 all-gather.12.cloned.1.call-start
  6.5 0.8 slice.57
  7.4 4.9 %collective-permute-start.1 = (s32[128]{0:T(128)S(1)}, s32[128]{0:T(128)S(1)}, u32[]{:S(2)}, u32[]{:S(2)}) collective-permute-start(s32[128]{0:T(128)S(1)} %slice.57), channel_id=1, source_target_pairs={{0,4},{4,8},{8,12},{12,16},{16,20},{20,24},{24,28},{1,5},{5,9},{9,... | collective-permute-start | bytes 1544 | tf_op jit(solution)/shard_map/ppermute | solution.py:17
  12.3 0.7 slice.58
  13.0 3.4 collective-permute-start.2
  16.4 0.7 slice.56
  17.1 3.4 collective-permute-start
  20.6 1.3 copy.17
  21.9 0.0 collective-permute-done.1
  21.9 0.7 pad_add_fusion
  22.6 1.4 fusion.21
  24.0 0.0 collective-permute-done.2
  24.0 0.0 copy-start.9
  24.0 2.6 fusion.1
  26.6 0.0 copy-done.9
  26.6 0.1 broadcast_maximum_fusion
  26.7 2.1 fusion
  28.8 0.1 exponential_add_fusion
  28.9 0.0 collective-permute-done
  28.9 0.0 copy-done.7
  28.9 3.1 fusion.22
  32.0 0.0 copy-done
  32.0 2.7 convolution_convert_fusion.2
  34.7 0.0 all-gather.12.cloned.1.call-update
  34.7 0.0 all-gather.6.cloned.1.call-start
  34.8 0.7 all-gather.6.cloned.1.call-update
  35.5 0.0 all-gather.8.cloned.1.call-start
  35.5 0.7 all-gather.8.cloned.1.call-update
  36.2 0.0 all-gather.10.cloned.1.call-start
  36.3 0.5 all-gather.10.cloned.1.call-update
  36.8 0.2 reduce-scatter.2.cloned.1.call-start
  37.0 0.0 copy-done.4
  37.0 0.0 copy-done.5
  37.0 0.1 slice_reduce_fusion.2
  37.1 0.1 slice.61
  37.2 0.0 copy-done.3
  37.2 0.1 pad_add_fusion.1
  37.3 55.1 %all-gather.12.cloned.1.call-done = bf16[2048,2048]{1,0:T(8,128)(2,1)} async-done(((bf16[512,2048]{1,0:T(8,128)(2,1)}), bf16[2048,2048]{1,0:T(8,128)(2,1)}) %all-gather.12.cloned.1.call-update) | async-done | bytes 8388624 | tf_op jit(solution)/shard_map/all_gather | solution.py:92
  92.4 7.3 %reduce_sum.58 = bf16[512,2048]{1,0:T(8,128)(2,1)} reduce(bf16[4,512,2048]{2,1,0:T(8,128)(2,1)} %bitcast.43, bf16[]{:T(256)} %constant.15.clone.1), dimensions={0}, to_apply=%region_2.3 | reduce | flops 3145728 | bytes 10485762 | tf_op jit(solution)/shard_map/reduce_sum | solution.py:92
  99.7 3.3 fusion.4
  103.0 0.0 copy-done.1
  103.0 0.7 copy-done.2
  103.7 1.0 multiply_reduce_fusion
  104.7 0.0 copy-done.6
  104.7 2.4 multiply_convert_fusion
  107.1 79.9 %all-gather.6.cloned.1.call-done = bf16[2048,1408]{1,0:T(8,128)(2,1)} async-done(((bf16[256,1408]{1,0:T(8,128)(2,1)}), bf16[2048,1408]{1,0:T(8,128)(2,1)}) %all-gather.6.cloned.1.call-update) | async-done | bytes 5767184 | tf_op jit(solution)/shard_map/all_gather | solution.py:104
  187.0 6.7 %convolution_convert_fusion.1 = bf16[512,1408]{1,0:T(8,128)(2,1)S(1)} fusion(bf16[512,2048]{1,0:T(8,128)(2,1)} %multiply_convert_fusion, bf16[2048,1408]{1,0:T(8,128)(2,1)} %all-gather.6.cloned.1.call-done), kind=kOutput, calls=%fused_computation.13 | convolution fusion | flops 2953510912 | bytes 9306112 | tf_op jit(solution)/shard_map/dot_general | solution.py:102
  193.7 0.0 copy-start.10
  193.7 1.1 copy-done.10
  194.8 2.5 collective-permute-start.3
  197.2 82.5 %all-gather.8.cloned.1.call-done = bf16[2048,1408]{1,0:T(8,128)(2,1)} async-done(((bf16[256,1408]{1,0:T(8,128)(2,1)}), bf16[2048,1408]{1,0:T(8,128)(2,1)}) %all-gather.8.cloned.1.call-update) | async-done | bytes 5767184 | tf_op jit(solution)/shard_map/all_gather | solution.py:109
  279.7 6.7 %convolution_convert_fusion = bf16[512,1408]{1,0:T(8,128)(2,1)S(1)} fusion(bf16[512,2048]{1,0:T(8,128)(2,1)} %multiply_convert_fusion, bf16[2048,1408]{1,0:T(8,128)(2,1)} %all-gather.8.cloned.1.call-done), kind=kOutput, calls=%fused_computation.12 | convolution fusion | flops 2953510912 | bytes 9306112 | tf_op jit(solution)/shard_map/dot_general | solution.py:107
  286.4 2.7 collective-permute-start.4
  289.1 0.1 slice_compare_fusion.1
  289.2 83.8 %all-gather.10.cloned.1.call-done = bf16[1408,2048]{1,0:T(8,128)(2,1)} async-done(((bf16[1408,256]{1,0:T(8,128)(2,1)}), bf16[1408,2048]{1,0:T(8,128)(2,1)}) %all-gather.10.cloned.1.call-update) | async-done | bytes 5767184 | tf_op jit(solution)/shard_map/all_gather | solution.py:124
  373.1 0.0 collective-permute-done.3
  373.1 0.0 collective-permute-done.4
  373.1 12.1 %convolution_convert_fusion.3 = bf16[512,2048]{1,0:T(8,128)(2,1)} fusion(bf16[1408,2048]{1,0:T(8,128)(2,1)} %all-gather.10.cloned.1.call-done, bf16[512,1408]{1,0:T(8,128)(2,1)} %copy-done.11, bf16[512,1408]{1,0:T(8,128)(2,1)} %copy-done.10, bf16[2,1408]{1,0:T(2,128)(2,1)S(1)} %collective-permute-done.4, bf16[2,1408]{1,0:T(2,128)(2,1)S(1)} %collective-permute-done.3, ...), kind=kOutput, calls=%fused_computation.15 | convolution fusion | flops 2984116224 | bytes 10793984 | tf_op jit(solution)/shard_map/dot_general | solution.py:122
  385.2 0.0 reduce-scatter.2.cloned.1.call-update
  385.2 29.5 %reduce-scatter.2.cloned.1.call-done = bf16[512,512]{1,0:T(8,128)(2,1)} async-done(((bf16[512,2048]{1,0:T(8,128)(2,1)}), bf16[512,512]{1,0:T(8,128)(2,1)}) %reduce-scatter.2.cloned.1.call-update) | async-done | bytes 524304 | tf_op jit(solution)/shard_map/reduce_scatter | solution.py:127
  414.7 1.5 fusion.25
  416.2 5.8 %all-reduce = (f32[512]{0:T(512)S(1)}, f32[512]{0:T(512)S(1)}) all-reduce(f32[512]{0:T(512)S(1)} %get-tuple-element.6, f32[512]{0:T(512)S(1)} %get-tuple-element.5), channel_id=1, replica_groups=mesh['sp'=8,'tp'=4] {'tp'}, use_global_device_ids=true, to_apply=%region_9.10 | all-reduce | flops 1024 | bytes 8192 | tf_op jit(solution)/shard_map/psum | solution.py:131
  422.0 2.3 multiply_convert_fusion.1
  (19 shorter events, 0.1 us)
Async XLA Ops:
  6.5 25.5 %copy-start = (bf16[512,2048]{1,0:T(8,128)(2,1)S(1)}, bf16[512,2048]{1,0:T(8,128)(2,1)}, u32[]{:S(2)}) copy-start(bf16[512,2048]{1,0:T(8,128)(2,1)} %param.20) | copy-start | bytes 6291460
  6.5 85.9 %all-gather.12.cloned.1.call-start = ((), (), s32[]{:S(2)}) async-start(), calls=%async_computation.5 | async-start | bytes 10485760 | tf_op jit(solution)/shard_map/all_gather | solution.py:92
  7.4 14.5 %collective-permute-start.1 = (s32[128]{0:T(128)S(1)}, s32[128]{0:T(128)S(1)}, u32[]{:S(2)}, u32[]{:S(2)}) collective-permute-start(s32[128]{0:T(128)S(1)} %slice.57), channel_id=1, source_target_pairs={{0,4},{4,8},{8,12},{12,16},{16,20},{20,24},{24,28},{1,5},{5,9},{9,... | collective-permute-start | bytes 1544 | tf_op jit(solution)/shard_map/ppermute | solution.py:17
  13.0 11.0 %collective-permute-start.2 = (bf16[128,64]{0,1:T(8,128)(2,1)S(1)}, bf16[128,64]{0,1:T(8,128)(2,1)S(1)}, u32[]{:S(2)}, u32[]{:S(2)}) collective-permute-start(bf16[128,64]{0,1:T(8,128)(2,1)S(1)} %slice.58), channel_id=1, source_target_pairs={{0,4},{4,8},{8,12},{12,16},{16,20},{20,24},{24,28},{1,5},{5,9},{9,... | collective-permute-start | bytes 49160 | tf_op jit(solution)/shard_map/ppermute | solution.py:17
  17.1 11.7 %collective-permute-start = (bf16[128,64]{0,1:T(8,128)(2,1)S(1)}, bf16[128,64]{0,1:T(8,128)(2,1)S(1)}, u32[]{:S(2)}, u32[]{:S(2)}) collective-permute-start(bf16[128,64]{0,1:T(8,128)(2,1)S(1)} %slice.56), channel_id=1, source_target_pairs={{0,4},{4,8},{8,12},{12,16},{16,20},{20,24},{24,28},{1,5},{5,9},{9,... | collective-permute-start | bytes 49160 | tf_op jit(solution)/shard_map/ppermute | solution.py:17
  24.0 2.6 copy-start.9
  26.7 2.2 copy-start.7
  34.7 2.3 copy-start.4
  34.7 2.3 copy-start.5
  34.7 2.5 copy-start.3
  34.7 152.2 %all-gather.6.cloned.1.call-start = ((), (), s32[]{:S(2)}) async-start(), calls=%async_computation.1 | async-start | bytes 6488064 | tf_op jit(solution)/shard_map/all_gather | solution.py:104
  35.5 244.2 %all-gather.8.cloned.1.call-start = ((), (), s32[]{:S(2)}) async-start(), calls=%async_computation.2 | async-start | bytes 6488064 | tf_op jit(solution)/shard_map/all_gather | solution.py:109
  36.2 336.8 %all-gather.10.cloned.1.call-start = ((), (), s32[]{:S(2)}) async-start(), calls=%async_computation.3 | async-start | bytes 6488064 | tf_op jit(solution)/shard_map/all_gather | solution.py:124
  36.8 377.9 %reduce-scatter.2.cloned.1.call-start = ((), (), s32[]{:S(2)}) async-start(), calls=%async_computation.4 | async-start | bytes 2621440 | tf_op jit(solution)/shard_map/reduce_scatter | solution.py:127
  99.7 3.3 copy-start.1
  99.7 4.0 copy-start.2
  102.9 1.7 copy-start.6
  193.7 1.1 copy-start.10
  194.8 178.3 %collective-permute-start.3 = (bf16[2,1408]{1,0:T(2,128)(2,1)S(1)}, bf16[2,1408]{1,0:T(2,128)(2,1)S(1)}, u32[]{:S(2)}, u32[]{:S(2)}) collective-permute-start(bf16[2,1408]{1,0:T(2,128)(2,1)S(1)} %slice.74), channel_id=1, source_target_pairs={{0,4},{4,8},{8,12},{12,16},{16,20},{20,24},{24,28},{1,5},{5,9},{9,... | collective-permute-start | bytes 16904 | tf_op jit(solution)/shard_map/ppermute | solution.py:17
  286.4 2.7 copy-start.11
  286.4 86.6 %collective-permute-start.4 = (bf16[2,1408]{1,0:T(2,128)(2,1)S(1)}, bf16[2,1408]{1,0:T(2,128)(2,1)S(1)}, u32[]{:S(2)}, u32[]{:S(2)}) collective-permute-start(bf16[2,1408]{1,0:T(2,128)(2,1)S(1)} %slice.77), channel_id=1, source_target_pairs={{0,4},{4,8},{8,12},{12,16},{16,20},{20,24},{24,28},{1,5},{5,9},{9,... | collective-permute-start | bytes 16904 | tf_op jit(solution)/shard_map/ppermute | solution.py:17
  385.2 36.8 %copy-start.8 = (f32[512]{0:T(512)S(1)}, f32[512]{0:T(512)}, u32[]{:S(2)}) copy-start(f32[512]{0:T(512)} %param.27) | copy-start | bytes 6148
Sparse Core Ops, SparseCore 0:
  34.9 57.5 all-gather.11
  94.6 92.3 all-gather.5
  189.2 90.5 all-gather.7
  281.6 91.3 all-gather.9
  385.3 29.3 reduce-scatter.1
